TPU v7x, 32 devices: a whole 2x2x4 slice. The times are simulated.
32 devices in a mesh: fs: 16 (over z, y, x), tp: 2 (over core).
Axes of the slice: x: 2, y: 2, z: 4, core: 2. Of those that a mesh axis runs over, the one named last changes fastest.
Arguments:
- tokens: bfloat16 [6144, 2048], P('fs'), may hold values from -6 to 6
- mixer_norm_gain: float32 [2048], replicated, may hold values from 0.1 to 1.9
- outer_gate_weight: bfloat16 [2048, 2048], P('fs', 'tp'), may hold values from -0.125 to 0.125
- inner_gate_weight: bfloat16 [2048, 2048], P('fs', 'tp'), may hold values from -0.125 to 0.125
- value_projection_weight: bfloat16 [2048, 2048], P('fs', 'tp'), may hold values from -0.125 to 0.125
- filter_taps_weight: float32 [3, 2048], replicated, may hold values from -3 to 3
- mixer_output_weight: bfloat16 [2048, 2048], P('tp', 'fs'), may hold values from -0.125 to 0.125
- feedforward_norm_gain: float32 [2048], replicated, may hold values from 0.1 to 1.9
- up_projection_weight: bfloat16 [2048, 8192], P('fs', 'tp'), may hold values from -0.125 to 0.125
- down_projection_weight: bfloat16 [8192, 2048], P('tp', 'fs'), may hold values from -0.0625 to 0.0625
Outputs:
- layer_out: bfloat16 [6144, 2048], P('fs')
All inputs are finite; a program needn't handle non-finite values.
Results may differ from a plain program's by a relative error of at most 0.02.
Values may be sent and summed in bfloat16 or wider, within the bound.
A program may use at most 128 MiB of HBM per device.

v0:
```python
import jax
import jax.numpy as jnp
from jax import lax
from jax.sharding import PartitionSpec as P


def rms_norm(rows, gain):
    floats = rows.astype(jnp.float32)
    scale = lax.rsqrt(jnp.mean(floats * floats, axis=-1, keepdims=True) + 1e-06)
    return (floats * scale * gain).astype(jnp.bfloat16)


def causal_mix(inner_product_rows, taps):
    length = inner_product_rows.shape[0]
    width = taps.shape[0]
    padded = jnp.pad(inner_product_rows, ((width - 1, 0), (0, 0)))
    total = jnp.zeros_like(inner_product_rows)
    for offset in range(width):
        total = total + taps[offset] * padded[offset : offset + length]
    return total


def settle(partial_value):
    rounded = lax.optimization_barrier(partial_value.astype(jnp.bfloat16))
    return rounded.astype(jnp.float32)


def on_device(
    tokens,
    mixer_norm_gain,
    outer_gate_weight,
    inner_gate_weight,
    value_projection_weight,
    filter_taps_weight,
    mixer_output_weight,
    feedforward_norm_gain,
    up_projection_weight,
    down_projection_weight,
):
    index = lax.axis_index("tp")
    local_width = outer_gate_weight.shape[1]
    first_normed_rows = rms_norm(tokens, mixer_norm_gain)
    pieces = (
        lax.all_gather(outer_gate_weight, "fs", axis=0, tiled=True),
        lax.all_gather(inner_gate_weight, "fs", axis=0, tiled=True),
        lax.all_gather(value_projection_weight, "fs", axis=0, tiled=True),
    )
    columns = first_normed_rows
    outer_gate_rows, inner_gate_rows, value_rows = tuple(
        (jnp.dot(columns, piece, preferred_element_type=jnp.float32) for piece in pieces)
    )
    outer_gate_rows = outer_gate_rows.astype(jnp.bfloat16)
    inner_gate_rows = inner_gate_rows.astype(jnp.bfloat16)
    value_rows = value_rows.astype(jnp.bfloat16)
    taps = lax.dynamic_slice_in_dim(filter_taps_weight, index * local_width, local_width, 1)
    inner_product_rows = inner_gate_rows.astype(jnp.float32) * value_rows.astype(jnp.float32)
    mixed = (outer_gate_rows.astype(jnp.float32) * causal_mix(inner_product_rows, taps)).astype(
        jnp.bfloat16
    )
    partial_value = settle(
        jnp.dot(
            mixed,
            lax.all_gather(mixer_output_weight, "fs", axis=1, tiled=True),
            preferred_element_type=jnp.float32,
        )
    )
    total = lax.psum(partial_value.astype(jnp.bfloat16), "tp").astype(jnp.float32)
    resid = (tokens.astype(jnp.float32) + total).astype(jnp.bfloat16)
    second = rms_norm(resid, feedforward_norm_gain)
    columns = second
    lifted = jnp.maximum(
        jnp.dot(
            columns,
            lax.all_gather(up_projection_weight, "fs", axis=0, tiled=True),
            preferred_element_type=jnp.float32,
        ),
        0.0,
    )
    hidden = (lifted * lifted).astype(jnp.bfloat16)
    down = jnp.dot(
        hidden,
        lax.all_gather(down_projection_weight, "fs", axis=1, tiled=True),
        preferred_element_type=jnp.float32,
    )
    total_down = lax.psum(settle(down).astype(jnp.bfloat16), "tp").astype(jnp.float32)
    return (resid.astype(jnp.float32) + total_down).astype(jnp.bfloat16)


def solution(mesh):
    return jax.shard_map(
        on_device,
        mesh=mesh,
        in_specs=(
            P("fs", None),
            P(),
            P("fs", "tp"),
            P("fs", "tp"),
            P("fs", "tp"),
            P(),
            P("tp", "fs"),
            P(),
            P("fs", "tp"),
            P("tp", "fs"),
        ),
        out_specs=P("fs", None),
        check_vma=False,
    )
```

profile of v0, /device:TPU:0, one launch (start us, length us, event | category | flops | bytes accessed | tf_op | source)
XLA Modules:
  0.0 859.7 jit_solution(13592114975854171140)
XLA Ops:
  6.5 0.7 all-gather.9.cloned.1.call-update
  7.3 0.0 all-gather.11.cloned.1.call-start
  7.3 0.7 all-gather.11.cloned.1.call-update
  8.0 0.0 all-gather.13.cloned.1.call-start
  8.1 0.7 all-gather.13.cloned.1.call-update
  8.7 0.0 all-gather.7.cloned.1.call-start
  8.8 0.5 all-gather.7.cloned.1.call-update
  9.3 0.0 all-reduce.4.cloned.1.call-start
  9.4 0.9 constant_dynamic-slice_fusion
  10.3 1.8 fusion.1
  12.1 0.0 copy-start.2
  12.1 76.3 %all-gather.9.cloned.1.call-done = bf16[2048,1024]{1,0:T(8,128)(2,1)} async-done(((bf16[128,1024]{1,0:T(8,128)(2,1)}), bf16[2048,1024]{1,0:T(8,128)(2,1)}) %all-gather.9.cloned.1.call-update) | async-done | bytes 4194320 | tf_op jit(solution)/shard_map/all_gather | solution.py:45
  88.4 4.5 convolution_convert_fusion.2
  93.0 72.5 %all-gather.11.cloned.1.call-done = bf16[2048,1024]{1,0:T(8,128)(2,1)} async-done(((bf16[128,1024]{1,0:T(8,128)(2,1)}), bf16[2048,1024]{1,0:T(8,128)(2,1)}) %all-gather.11.cloned.1.call-update) | async-done | bytes 4194320 | tf_op jit(solution)/shard_map/all_gather | solution.py:46
  165.4 5.2 convert_multiply_fusion.4
  170.6 84.9 %all-gather.13.cloned.1.call-done = bf16[1024,2048]{1,0:T(8,128)(2,1)} async-done(((bf16[1024,128]{1,0:T(8,128)(2,1)}), bf16[1024,2048]{1,0:T(8,128)(2,1)}) %all-gather.13.cloned.1.call-update) | async-done | bytes 4194320 | tf_op jit(solution)/shard_map/all_gather | solution.py:63
  255.5 76.4 %all-gather.7.cloned.1.call-done = bf16[2048,1024]{1,0:T(8,128)(2,1)} async-done(((bf16[128,1024]{1,0:T(8,128)(2,1)}), bf16[2048,1024]{1,0:T(8,128)(2,1)}) %all-gather.7.cloned.1.call-update) | async-done | bytes 4194320 | tf_op jit(solution)/shard_map/all_gather | solution.py:44
  331.9 9.9 %convolution_convert_fusion = bf16[384,2048]{1,0:T(8,128)(2,1)} fusion(bf16[1024,2048]{1,0:T(8,128)(2,1)} %all-gather.13.cloned.1.call-done, f32[384,1024]{1,0:T(8,128)} %convert_multiply_fusion.4, bf16[2048,1024]{1,0:T(8,128)(2,1)} %all-gather.7.cloned.1.call-done, f32[1024]{0:T(1024)S(1)} %bitcast.11, f32[1024]{0:T(1024)S(1)} %bitcast.10, ...), kind=kOutput, calls=%fused_computation.18 | convolution fusion | flops 3228696576 | bytes 13129216 | tf_op jit(solution)/shard_map/dot_general | solution.py:61
  341.8 0.0 all-reduce.4.cloned.1.call-update
  341.8 0.0 all-gather.15.cloned.1.call-start
  341.9 0.5 all-gather.15.cloned.1.call-update
  342.4 0.0 all-gather.17.cloned.1.call-start
  342.5 0.7 all-gather.17.cloned.1.call-update
  343.2 0.2 all-reduce.6.cloned.1.call-start
  343.4 17.6 %all-reduce.4.cloned.1.call-done = bf16[384,2048]{1,0:T(8,128)(2,1)} async-done(((bf16[384,2048]{1,0:T(8,128)(2,1)}), bf16[384,2048]{1,0:T(8,128)(2,1)}) %all-reduce.4.cloned.1.call-update) | async-done | bytes 1572880 | tf_op jit(solution)/shard_map/psum | solution.py:67
  361.0 2.1 fusion.5
  363.1 192.7 %all-gather.15.cloned.1.call-done = bf16[2048,4096]{1,0:T(8,128)(2,1)} async-done(((bf16[128,4096]{1,0:T(8,128)(2,1)}), bf16[2048,4096]{1,0:T(8,128)(2,1)}) %all-gather.15.cloned.1.call-update) | async-done | bytes 16777232 | tf_op jit(solution)/shard_map/all_gather | solution.py:74
  555.8 250.0 %all-gather.17.cloned.1.call-done = bf16[4096,2048]{1,0:T(8,128)(2,1)} async-done(((bf16[4096,128]{1,0:T(8,128)(2,1)}), bf16[4096,2048]{1,0:T(8,128)(2,1)}) %all-gather.17.cloned.1.call-update) | async-done | bytes 16777232 | tf_op jit(solution)/shard_map/all_gather | solution.py:82
  805.8 24.9 %fusion.10 = bf16[384,2048]{1,0:T(8,128)(2,1)} fusion(bf16[4096,2048]{1,0:T(8,128)(2,1)} %all-gather.17.cloned.1.call-done, bf16[2048,4096]{1,0:T(8,128)(2,1)} %all-gather.15.cloned.1.call-done, f32[2048]{0:T(1024)S(1)} %copy-done.3, f32[384]{0:T(512)S(1)} %add_rsqrt_fusion, bf16[384,2048]{1,0:T(8,128)(2,1)S(1)} %copy-done, bf16[384,2048]{1,0:T(8,128)(2,1)S(1)} %copy-done.1), kind=kOutput, calls=%fused_computation.17 | convolution fusion | flops 12896698368 | bytes 38282752 | tf_op jit(solution)/shard_map/dot_general | solution.py:80
  830.8 0.0 all-reduce.6.cloned.1.call-update
  830.8 18.7 %all-reduce.6.cloned.1.call-done = bf16[384,2048]{1,0:T(8,128)(2,1)} async-done(((bf16[384,2048]{1,0:T(8,128)(2,1)}), bf16[384,2048]{1,0:T(8,128)(2,1)}) %all-reduce.6.cloned.1.call-update) | async-done | bytes 1572880 | tf_op jit(solution)/shard_map/psum | solution.py:85
  849.5 3.4 fusion.8
  (10 shorter events, 0.0 us)
Async XLA Ops:
  6.5 81.9 %all-gather.9.cloned.1.call-start = ((), (), s32[]{:S(2)}) async-start(), calls=%async_computation.1 | async-start | bytes 4456448 | tf_op jit(solution)/shard_map/all_gather | solution.py:45
  7.3 158.2 %all-gather.11.cloned.1.call-start = ((), (), s32[]{:S(2)}) async-start(), calls=%async_computation.2 | async-start | bytes 4456448 | tf_op jit(solution)/shard_map/all_gather | solution.py:46
  8.0 247.5 %all-gather.13.cloned.1.call-start = ((), (), s32[]{:S(2)}) async-start(), calls=%async_computation.3 | async-start | bytes 4456448 | tf_op jit(solution)/shard_map/all_gather | solution.py:63
  8.7 323.2 %all-gather.7.cloned.1.call-start = ((), (), s32[]{:S(2)}) async-start(), calls=%async_computation | async-start | bytes 4456448 | tf_op jit(solution)/shard_map/all_gather | solution.py:44
  9.3 351.6 %all-reduce.4.cloned.1.call-start = ((), (), s32[]{:S(2)}) async-start(), calls=%async_computation.4 | async-start | bytes 3145728 | tf_op jit(solution)/shard_map/psum | solution.py:67
  12.1 153.3 %copy-start = (bf16[384,2048]{1,0:T(8,128)(2,1)S(1)}, bf16[384,2048]{1,0:T(8,128)(2,1)}, u32[]{:S(2)}) copy-start(bf16[384,2048]{1,0:T(8,128)(2,1)} %param.10) | copy-start | bytes 4718596
  12.1 153.3 %copy-start.2 = (f32[2048]{0:T(1024)S(1)}, f32[2048]{0:T(1024)}, u32[]{:S(2)}) copy-start(f32[2048]{0:T(1024)} %param.11) | copy-start | bytes 24580
  341.8 464.0 %copy-start.3 = (f32[2048]{0:T(1024)S(1)}, f32[2048]{0:T(1024)}, u32[]{:S(2)}) copy-start(f32[2048]{0:T(1024)} %param.17) | copy-start | bytes 24580
  341.8 214.0 %all-gather.15.cloned.1.call-start = ((), (), s32[]{:S(2)}) async-start(), calls=%async_computation.5 | async-start | bytes 17825792 | tf_op jit(solution)/shard_map/all_gather | solution.py:74
  342.4 463.4 %all-gather.17.cloned.1.call-start = ((), (), s32[]{:S(2)}) async-start(), calls=%async_computation.6 | async-start | bytes 17825792 | tf_op jit(solution)/shard_map/all_gather | solution.py:82
  343.2 506.3 %all-reduce.6.cloned.1.call-start = ((), (), s32[]{:S(2)}) async-start(), calls=%async_computation.7 | async-start | bytes 3145728 | tf_op jit(solution)/shard_map/psum | solution.py:85
  361.0 444.9 %copy-start.1 = (bf16[384,2048]{1,0:T(8,128)(2,1)S(1)}, bf16[384,2048]{1,0:T(8,128)(2,1)}, u32[]{:S(2)}) copy-start(bf16[384,2048]{1,0:T(8,128)(2,1)} %all-reduce.4.cloned.1.call-done) | copy-start | bytes 4718596
Sparse Core Ops, SparseCore 0:
  10.1 78.3 all-gather.8
  91.2 74.1 all-gather.10
  168.1 87.3 all-gather.12
  258.1 73.7 all-gather.6
  342.0 18.9 all-reduce.3
  363.6 192.1 all-gather.14
  558.5 247.2 all-gather.16
  830.9 18.5 all-reduce.5
where the time goes:
time: 860 us
  waiting for transfers between devices  793 us (92%)
  matrix products  44.5 us (5%)
  between operations  13.5 us (2%)
    all_gather x1, waiting for transfers between devices, on_device(): lax.all_gather(down_projection_weight, 'fs', axis=1, tiled=True)  250 us
    all_gather x1, waiting for transfers between devices, on_device(): lax.all_gather(up_projection_weight, 'fs', axis=0, tiled=True)  193 us
    all_gather x1, waiting for transfers between devices, on_device(): lax.all_gather(mixer_output_weight, 'fs', axis=1, tiled=True)  84.9 us
    all_gather x1, waiting for transfers between devices, on_device(): lax.all_gather(outer_gate_weight, 'fs', axis=0, tiled=True)  76.4 us
    all_gather x1, waiting for transfers between devices, on_device(): lax.all_gather(inner_gate_weight, 'fs', axis=0, tiled=True)  76.3 us
    all_gather x1, waiting for transfers between devices, on_device(): lax.all_gather(value_projection_weight, 'fs', axis=0, tiled=True)  72.5 us
    dot_general x1, matrix products, on_device(): jnp.dot(hidden, lax.all_gather(down_projection_weight, 'fs', axis=1, tile...  24.9 us
    psum x1, waiting for transfers between devices, on_device(): lax.psum(settle(down).astype(jnp.bfloat16), 'tp').astype(jnp.float32)  18.7 us
  transfers between devices with their start and end apart: 8, of which 8 were waited for; matrix products, arithmetic and copies ran while one was open for 2% of the time, Pallas kernels for 0%

commit v1 on v0

--- a/solution.py
+++ b/solution.py
@@ -1,6 +1,10 @@
+import functools
+
 import jax
 import jax.numpy as jnp
 from jax import lax
+from jax.experimental import pallas as pl
+from jax.experimental.pallas import tpu as pltpu
 from jax.sharding import PartitionSpec as P
 
 
@@ -86,9 +90,532 @@
     return (resid.astype(jnp.float32) + total_down).astype(jnp.bfloat16)
 
 
+MESH = pl.DeviceIdType.MESH
+CAST = 4
+STRIP = 64
+
+
+def fused_kernel(
+    planes,
+    tokens,
+    gain_one,
+    w_outer,
+    w_inner,
+    w_value,
+    taps,
+    w_mix,
+    gain_two,
+    w_up,
+    w_down,
+    out,
+    proj,
+    mix,
+    up,
+    down,
+    gathered,
+    normed,
+    hidden,
+    part,
+    pair_one,
+    pair_two,
+    cross_one,
+    cross_two,
+    resid,
+    swap_send,
+    swap_recv,
+    chain_send,
+    chain_recv,
+    tok_send,
+    tok_recv,
+    fwd_send,
+    fwd_recv,
+    sec_send,
+    sec_recv,
+    secf_send,
+    secf_recv,
+    pair_send,
+    pair_recv,
+    cross_send,
+    cross_recv,
+    last_send,
+    last_recv,
+):
+    f = lax.axis_index("fs")
+    t = lax.axis_index("tp")
+    g = f // CAST
+    j = lax.rem(f, CAST)
+    rows = tokens.shape[0]
+    half = rows // 2
+    depth = w_outer.shape[0]
+    wide = w_outer.shape[1] // CAST
+    tall = w_up.shape[1] // CAST
+    width = tokens.shape[1]
+    mine = pl.multiple_of(t * half, half)
+    other = pl.multiple_of((1 - t) * half, half)
+
+    def peer(i):
+        return lax.rem(j + i, CAST)
+
+    def at(plane, k, core):
+        return {"fs": plane * CAST + k, "tp": core}
+
+    partner = at(g, j, 1 - t)
+
+    def remote(src, dst, send, recv, device):
+        return pltpu.make_async_remote_copy(
+            src_ref=src,
+            dst_ref=dst,
+            send_sem=send,
+            recv_sem=recv,
+            device_id=device,
+            device_id_type=MESH,
+        )
+
+    barrier = pltpu.get_barrier_semaphore()
+    for i in range(1, CAST):
+        pl.semaphore_signal(barrier, inc=1, device_id=at(g, peer(i), t), device_id_type=MESH)
+    pl.semaphore_signal(barrier, inc=1, device_id=partner, device_id_type=MESH)
+
+    @pl.when(g > 0)
+    def _():
+        pl.semaphore_signal(barrier, inc=1, device_id=at(g - 1, j, t), device_id_type=MESH)
+
+    @pl.when(g < planes - 1)
+    def _():
+        pl.semaphore_signal(barrier, inc=1, device_id=at(g + 1, j, t), device_id_type=MESH)
+
+    ends = jnp.minimum(g, 1) + jnp.minimum(planes - 1 - g, 1)
+    pl.semaphore_wait(barrier, CAST + ends)
+
+    def lanes(start, size):
+        return pl.ds(pl.multiple_of(start, 128), size)
+
+    shards = (w_outer, w_inner, w_value, w_mix, w_up, w_down)
+
+    def block(kind, k):
+        if kind < 3:
+            return shards[kind].at[:, lanes(k * wide, wide)]
+        if kind == 3:
+            return w_mix.at[pl.ds(pl.multiple_of(k * wide, wide), wide), :]
+        if kind == 4:
+            return w_up.at[:, lanes(k * tall, tall)]
+        return w_down.at[pl.ds(pl.multiple_of(k * tall, tall), tall), :]
+
+    def place(kind, owner):
+        start = pl.multiple_of(owner * depth, depth)
+        if kind < 3:
+            return proj.at[pl.ds(start, depth), pl.ds(kind * wide, wide)]
+        if kind == 3:
+            return mix.at[:, lanes(owner * depth, depth)]
+        if kind == 4:
+            return up.at[pl.ds(start, depth), :]
+        return down.at[:, lanes(owner * depth, depth)]
+
+    def swap(kind, i):
+        k = peer(i)
+        return remote(
+            block(kind, k),
+            place(kind, f),
+            swap_send.at[kind, i],
+            swap_recv.at[kind, j],
+            at(g, k, t),
+        )
+
+    def swap_local(kind):
+        return pltpu.make_async_copy(block(kind, j), place(kind, f), swap_recv.at[kind, j])
+
+    def start_swap(kind):
+        for i in range(1, CAST):
+            swap(kind, i).start()
+        swap_local(kind).start()
+
+    def wait_swap(kind, k):
+        pltpu.make_async_copy(
+            place(kind, g * CAST + k), place(kind, g * CAST + k), swap_recv.at[kind, k]
+        ).wait()
+
+    chunks = [(kind, None) for kind in range(4)]
+    chunks += [(4, q) for q in range(CAST)] + [(5, q) for q in range(CAST)]
+
+    def slab(w, plane):
+        kind, q = chunks[w]
+        if q is not None:
+            return place(kind, plane * CAST + q)
+        start = pl.multiple_of(plane * CAST * depth, CAST * depth)
+        if kind < 3:
+            return proj.at[pl.ds(start, CAST * depth), pl.ds(kind * wide, wide)]
+        return mix.at[:, lanes(plane * CAST * depth, CAST * depth)]
+
+    def hop(w, plane, up_way):
+        return remote(
+            slab(w, plane),
+            slab(w, plane),
+            chain_send.at[w, plane, 1 if up_way else 0],
+            chain_recv.at[w, plane],
+            at(g + 1 if up_way else g - 1, j, t),
+        )
+
+    def pump(step):
+        for dist in range(planes):
+            w = step - dist
+            if w < 0 or w >= len(chunks):
+                continue
+            if dist == 0:
+                kind, q = chunks[w]
+                for k in range(CAST) if q is None else (q,):
+                    wait_swap(kind, k)
+
+                @pl.when(g < planes - 1)
+                def _():
+                    hop(w, g, True).start()
+
+                @pl.when(g > 0)
+                def _():
+                    hop(w, g, False).start()
+
+            else:
+
+                @pl.when(g - dist >= 0)
+                def _():
+                    source = g - dist
+                    pltpu.make_async_copy(
+                        slab(w, source), slab(w, source), chain_recv.at[w, source]
+                    ).wait()
+
+                    @pl.when(g < planes - 1)
+                    def _():
+                        hop(w, source, True).start()
+
+                @pl.when(g + dist < planes)
+                def _():
+                    source = g + dist
+                    pltpu.make_async_copy(
+                        slab(w, source), slab(w, source), chain_recv.at[w, source]
+                    ).wait()
+
+                    @pl.when(g > 0)
+                    def _():
+                        hop(w, source, False).start()
+
+    def drain():
+        for kind in range(6):
+            for i in range(1, CAST):
+                swap(kind, i).wait_send()
+        for w in range(len(chunks)):
+            for plane in range(planes):
+
+                @pl.when(jnp.logical_and(g >= plane, g < planes - 1))
+                def _():
+                    hop(w, plane, True).wait_send()
+
+                @pl.when(jnp.logical_and(g <= plane, g > 0))
+                def _():
+                    hop(w, plane, False).wait_send()
+
+    def spread(source, i, send, recv):
+        return remote(
+            source, gathered.at[j, pl.ds(mine, half)], send.at[i], recv.at[i], at(g, peer(i), t)
+        )
+
+    def landed(i):
+        return gathered.at[lax.rem(j + CAST - i, CAST), pl.ds(mine, half)]
+
+    def relay(i, send, recv):
+        return remote(landed(i), landed(i), send.at[i], recv.at[i], partner)
+
+    def relayed(i, recv):
+        ref = gathered.at[lax.rem(j + CAST - i, CAST), pl.ds(other, half)]
+        return pltpu.make_async_copy(ref, ref, recv.at[i])
+
+    def arrived(i, recv):
+        return pltpu.make_async_copy(landed(i), landed(i), recv.at[i])
+
+    def norm(x, gain):
+        floats = x.astype(jnp.float32)
+        scale = lax.rsqrt(jnp.mean(floats * floats, axis=-1, keepdims=True) + 1e-06)
+        return (floats * scale * gain).astype(jnp.bfloat16)
+
+    own = tokens.at[pl.ds(mine, half)]
+    for kind in range(4):
+        start_swap(kind)
+    for i in range(1, CAST):
+        spread(own, i, tok_send, tok_recv).start()
+    for kind in (4, 5):
+        start_swap(kind)
+    keep = pltpu.make_async_copy(tokens, gathered.at[j], tok_recv.at[0])
+    keep.start()
+
+    for step in range(3):
+        pump(step)
+    for i in range(1, CAST):
+        arrived(i, tok_recv).wait()
+        relay(i, fwd_send, fwd_recv).start()
+    pump(3)
+    for i in range(1, CAST):
+        spread(own, i, tok_send, tok_recv).wait_send()
+        relay(i, fwd_send, fwd_recv).wait_send()
+        relayed(i, fwd_recv).wait()
+    keep.wait()
+    for step in range(4, 4 + planes - 1):
+        pump(step)
+    done = 4 + planes - 1
+    total = len(chunks) + planes - 1
+
+    channel = lanes((t * CAST + j) * wide, wide)
+    dims = (((1,), (0,)), ((), ()))
+
+    def dot(a, b):
+        return lax.dot_general(a, b, dims, preferred_element_type=jnp.float32)
+
+    def mixer(s):
+        @pl.loop(0, rows // STRIP)
+        def _(r):
+            at_rows = pl.ds(pl.multiple_of(r * STRIP, STRIP), STRIP)
+            normed[at_rows, :] = norm(gathered[s, at_rows, :], gain_one[...])
+
+        x = normed[...]
+        outer = dot(x, proj[:, 0:wide]).astype(jnp.bfloat16).astype(jnp.float32)
+        carrier = dot(x, proj[:, wide : 2 * wide]).astype(jnp.bfloat16).astype(jnp.float32)
+        values = dot(x, proj[:, 2 * wide : 3 * wide]).astype(jnp.bfloat16).astype(jnp.float32)
+        inner = carrier * values
+        count = taps.shape[0]
+        position = lax.broadcasted_iota(jnp.int32, inner.shape, 0)
+        conv = taps[count - 1 : count, channel] * inner
+        for back in range(1, count):
+            moved = jnp.where(position >= back, pltpu.roll(inner, back, 0), 0.0)
+            conv = conv + taps[count - 1 - back : count - back, channel] * moved
+        mixed = (outer * conv).astype(jnp.bfloat16)
+        for n in range(0, width, 512):
+            part[s, :, n : n + 512] = dot(mixed, mix[:, n : n + 512]).astype(jnp.bfloat16)
+
+    def feed_up(s):
+        for n in range(0, tall, 256):
+            lifted = jnp.maximum(dot(gathered[s], up[:, n : n + 256]), 0.0)
+            hidden[s, :, n : n + 256] = (lifted * lifted).astype(jnp.bfloat16)
+
+    def feed_down(s):
+        for n in range(0, width, 256):
+            part[s, :, n : n + 256] = dot(hidden[s], down[:, n : n + 256]).astype(jnp.bfloat16)
+
+    def pair(turn, i, buffer):
+        s = peer(i)
+        return remote(
+            part.at[s, pl.ds(other, half)],
+            buffer.at[s],
+            pair_send.at[turn, i],
+            pair_recv.at[turn, i],
+            partner,
+        )
+
+    def pair_wait(turn, i, buffer):
+        s = peer(i)
+        pltpu.make_async_copy(buffer.at[s], buffer.at[s], pair_recv.at[turn, i]).wait()
+
+    def cross(turn, i, buffer, target):
+        return remote(
+            buffer.at[peer(i)],
+            target.at[i - 1],
+            cross_send.at[turn, i],
+            cross_recv.at[turn, i],
+            at(g, peer(i), t),
+        )
+
+    def cross_wait(turn, i, target):
+        ref = target.at[i - 1]
+        pltpu.make_async_copy(ref, ref, cross_recv.at[turn, i]).wait()
+
+    def strip(r, start=0):
+        return pl.ds(pl.multiple_of(start + r * STRIP, STRIP), STRIP)
+
+    def add_pair(i, buffer):
+        s = peer(i)
+
+        @pl.loop(0, half // STRIP)
+        def _(r):
+            a = part[s, strip(r, mine), :].astype(jnp.float32)
+            buffer[s, strip(r), :] = (a + buffer[s, strip(r), :].astype(jnp.float32)).astype(
+                jnp.bfloat16
+            )
+
+    def add_cross(r, buffer, target):
+        value = buffer[j, strip(r), :].astype(jnp.float32)
+        for i in range(CAST - 1):
+            value = value + target[i, strip(r), :].astype(jnp.float32)
+        return value
+
+    order = list(range(1, CAST)) + [0]
+    for i in order:
+        mixer(peer(i))
+        pair(0, i, pair_one).start()
+        if i == 2:
+            pump(done)
+    pump(done + 1)
+    for i in order:
+        pair_wait(0, i, pair_one)
+        add_pair(i, pair_one)
+        if i:
+            cross(0, i, pair_one, cross_one).start()
+    pump(done + 2)
+    for i in range(1, CAST):
+        cross_wait(0, i, cross_one)
+
+    @pl.loop(0, half // STRIP)
+    def _(r):
+        total_mix = add_cross(r, pair_one, cross_one)
+        row = tokens[strip(r, mine), :].astype(jnp.float32) + total_mix
+        row = row.astype(jnp.bfloat16)
+        resid[strip(r), :] = row
+        gathered[j, strip(r, mine), :] = norm(row, gain_two[...])
+
+    fresh = gathered.at[j, pl.ds(mine, half)]
+    for i in range(1, CAST):
+        spread(fresh, i, sec_send, sec_recv).start()
+    relay(0, secf_send, secf_recv).start()
+    for i in order:
+        pair(0, i, pair_one).wait_send()
+        if i:
+            cross(0, i, pair_one, cross_one).wait_send()
+    pump(done + 3)
+    for i in range(1, CAST):
+        arrived(i, sec_recv).wait()
+        relay(i, secf_send, secf_recv).start()
+    pump(done + 4)
+    for i in order:
+        relayed(i, secf_recv).wait()
+    for i in order:
+        feed_up(peer(i))
+    for step in range(done + 5, total):
+        pump(step)
+    for i in order:
+        feed_down(peer(i))
+        pair(1, i, pair_two).start()
+    for i in order:
+        pair_wait(1, i, pair_two)
+        add_pair(i, pair_two)
+        if i:
+            cross(1, i, pair_two, cross_two).start()
+    drain()
+    for i in range(1, CAST):
+        spread(fresh, i, sec_send, sec_recv).wait_send()
+    for i in order:
+        relay(i, secf_send, secf_recv).wait_send()
+    for i in range(1, CAST):
+        cross_wait(1, i, cross_two)
+
+    @pl.loop(0, half // STRIP)
+    def _(r):
+        value = resid[strip(r), :].astype(jnp.float32) + add_cross(r, pair_two, cross_two)
+        out[strip(r, mine), :] = value.astype(jnp.bfloat16)
+
+    final = remote(
+        out.at[pl.ds(mine, half)],
+        out.at[pl.ds(mine, half)],
+        last_send.at[0],
+        last_recv.at[0],
+        partner,
+    )
+    final.start()
+    for i in order:
+        pair(1, i, pair_two).wait_send()
+        if i:
+            cross(1, i, pair_two, cross_two).wait_send()
+    final.wait()
+
+
+def fused(
+    tokens,
+    mixer_norm_gain,
+    outer_gate_weight,
+    inner_gate_weight,
+    value_projection_weight,
+    filter_taps_weight,
+    mixer_output_weight,
+    feedforward_norm_gain,
+    up_projection_weight,
+    down_projection_weight,
+):
+    rows, width = tokens.shape
+    half = rows // 2
+    planes = width // (outer_gate_weight.shape[0] * CAST)
+    wide = outer_gate_weight.shape[1] // CAST
+    tall = up_projection_weight.shape[1] // CAST
+    dma = pltpu.SemaphoreType.DMA
+    chunk_count = 4 + 2 * CAST
+    bf16 = jnp.bfloat16
+    return pl.pallas_call(
+        functools.partial(fused_kernel, planes),
+        out_shape=jax.ShapeDtypeStruct((rows, width), bf16),
+        in_specs=[pl.BlockSpec(memory_space=pltpu.VMEM)] * 10,
+        out_specs=pl.BlockSpec(memory_space=pltpu.VMEM),
+        scratch_shapes=[
+            pltpu.VMEM((width, 3 * wide), bf16),
+            pltpu.VMEM((wide, width), bf16),
+            pltpu.VMEM((width, tall), bf16),
+            pltpu.VMEM((tall, width), bf16),
+            pltpu.VMEM((CAST, rows, width), bf16),
+            pltpu.VMEM((rows, width), bf16),
+            pltpu.VMEM((CAST, rows, tall), bf16),
+            pltpu.VMEM((CAST, rows, width), bf16),
+            pltpu.VMEM((CAST, half, width), bf16),
+            pltpu.VMEM((CAST, half, width), bf16),
+            pltpu.VMEM((CAST - 1, half, width), bf16),
+            pltpu.VMEM((CAST - 1, half, width), bf16),
+            pltpu.VMEM((half, width), bf16),
+            dma((6, CAST)),
+            dma((6, CAST)),
+            dma((chunk_count, planes, 2)),
+            dma((chunk_count, planes)),
+            dma((CAST,)),
+            dma((CAST,)),
+            dma((CAST,)),
+            dma((CAST,)),
+            dma((CAST,)),
+            dma((CAST,)),
+            dma((CAST,)),
+            dma((CAST,)),
+            dma((2, CAST)),
+            dma((2, CAST)),
+            dma((2, CAST)),
+            dma((2, CAST)),
+            dma((1,)),
+            dma((1,)),
+        ],
+        compiler_params=pltpu.CompilerParams(
+            collective_id=1, has_side_effects=True, vmem_limit_bytes=63 * 1024 * 1024
+        ),
+        name="fused_layer",
+    )(
+        tokens,
+        mixer_norm_gain.reshape(1, -1),
+        outer_gate_weight,
+        inner_gate_weight,
+        value_projection_weight,
+        filter_taps_weight,
+        mixer_output_weight,
+        feedforward_norm_gain.reshape(1, -1),
+        up_projection_weight,
+        down_projection_weight,
+    )
+
+
+def layer(*args):
+    tokens, outer, up = args[0], args[2], args[8]
+    depth = outer.shape[0]
+    fits = (
+        lax.axis_size("tp") == 2
+        and lax.axis_size("fs") % CAST == 0
+        and depth % 128 == 0
+        and outer.shape[1] % (CAST * 128) == 0
+        and up.shape[1] % (CAST * 256) == 0
+        and tokens.shape[0] % (2 * STRIP) == 0
+        and tokens.shape[1] % 512 == 0
+    )
+    return fused(*args) if fits else on_device(*args)
+
+
 def solution(mesh):
     return jax.shard_map(
-        on_device,
+        layer,
         mesh=mesh,
         in_specs=(
             P("fs", None),

time: 860 us -> 274 us (0.32)
  waiting for transfers between devices: 793 us -> 0 us
  Pallas kernels: 0 us -> 271 us
  matrix products: 44.5 us -> 0 us
  between operations: 13.5 us -> 0.01 us
    all_gather x6 -> x0, waiting for transfers between devices: 753 us -> none  [the longest x1 250 us: on_device(): lax.all_gather(down_projection_weight, 'fs', axis=1, tiled=True)]
    pallas_call x0 -> x1, Pallas kernels: none -> 271 us  [fused(): pl.pallas_call(functools.partial(fused_kernel, planes), out_shape=jax.Sha...]
    dot_general x4 -> x0, matrix products: 44.5 us -> none  [the longest x1 24.9 us: on_device(): jnp.dot(hidden, lax.all_gather(down_projection_weight, 'fs', axis=1, tile...]
    psum x2 -> x0, waiting for transfers between devices: 36.3 us -> none  [the longest x1 18.7 us: on_device(): lax.psum(settle(down).astype(jnp.bfloat16), 'tp').astype(jnp.float32)]
  transfers between devices with their start and end apart: 8 -> 0, of which waited for: 8 -> 0; matrix products, arithmetic and copies ran while one was open for 2% -> 0% of each run, Pallas kernels for 0% -> 0%
where the time goes in v1:
time: 274 us
  Pallas kernels  271 us (99%)
    pallas_call x1, Pallas kernels, fused(): pl.pallas_call(functools.partial(fused_kernel, planes), out_shape=jax.Sha...  271 us

profile of v1, /device:TPU:0, one launch (start us, length us, event | category | flops | bytes accessed | tf_op | source)
XLA Modules:
  0.0 274.0 jit_solution(15425337737476829777)
XLA Ops:
  0.0 271.3 %fused_layer.1 = bf16[384,2048]{1,0:T(8,128)(2,1)} custom-call(bf16[384,2048]{1,0:T(8,128)(2,1)} %tokens.1, f32[1,2048]{1,0:T(1,128)} %bitcast.2, bf16[128,1024]{1,0:T(8,128)(2,1)} %w_outer.1, bf16[128,1024]{1,0:T(8,128)(2,1)} %w_inner.1, bf16[128,1024]{1,0:T(8,128)(2,1)} %w_value.1, f32[3,2048]{1,0:T(4,128)} %taps.1, bf16[1024,128]{1,0:T(8,128)(2,1)} %w_mix.1, ...), custom_call_target="tpu_custom_call" | custom-call | tf_op jit(solution)/shard_map/fused_layer/pallas_call | solution.py:545
  271.3 2.7 copy.12

commit v2 on v1

--- a/solution.py
+++ b/solution.py
@@ -137,6 +137,8 @@
     pair_recv,
     cross_send,
     cross_recv,
+    set_send,
+    set_recv,
     last_send,
     last_recv,
 ):
@@ -201,7 +203,8 @@
             return w_up.at[:, lanes(k * tall, tall)]
         return w_down.at[pl.ds(pl.multiple_of(k * tall, tall), tall), :]
 
-    def place(kind, owner):
+    def place(kind, plane, k):
+        owner = plane * CAST + k
         start = pl.multiple_of(owner * depth, depth)
         if kind < 3:
             return proj.at[pl.ds(start, depth), pl.ds(kind * wide, wide)]
@@ -209,20 +212,20 @@
             return mix.at[:, lanes(owner * depth, depth)]
         if kind == 4:
             return up.at[pl.ds(start, depth), :]
-        return down.at[:, lanes(owner * depth, depth)]
+        return down.at[k, :, lanes(plane * depth, depth)]
 
     def swap(kind, i):
         k = peer(i)
         return remote(
             block(kind, k),
-            place(kind, f),
+            place(kind, g, j),
             swap_send.at[kind, i],
             swap_recv.at[kind, j],
             at(g, k, t),
         )
 
     def swap_local(kind):
-        return pltpu.make_async_copy(block(kind, j), place(kind, f), swap_recv.at[kind, j])
+        return pltpu.make_async_copy(block(kind, j), place(kind, g, j), swap_recv.at[kind, j])
 
     def start_swap(kind):
         for i in range(1, CAST):
@@ -231,7 +234,7 @@
 
     def wait_swap(kind, k):
         pltpu.make_async_copy(
-            place(kind, g * CAST + k), place(kind, g * CAST + k), swap_recv.at[kind, k]
+            place(kind, g, k), place(kind, g, k), swap_recv.at[kind, k]
         ).wait()
 
     chunks = [(kind, None) for kind in range(4)]
@@ -240,7 +243,7 @@
     def slab(w, plane):
         kind, q = chunks[w]
         if q is not None:
-            return place(kind, plane * CAST + q)
+            return place(kind, plane, q)
         start = pl.multiple_of(plane * CAST * depth, CAST * depth)
         if kind < 3:
             return proj.at[pl.ds(start, CAST * depth), pl.ds(kind * wide, wide)]
@@ -359,7 +362,6 @@
     for step in range(4, 4 + planes - 1):
         pump(step)
     done = 4 + planes - 1
-    total = len(chunks) + planes - 1
 
     channel = lanes((t * CAST + j) * wide, wide)
     dims = (((1,), (0,)), ((), ()))
@@ -393,9 +395,66 @@
             lifted = jnp.maximum(dot(gathered[s], up[:, n : n + 256]), 0.0)
             hidden[s, :, n : n + 256] = (lifted * lifted).astype(jnp.bfloat16)
 
-    def feed_down(s):
-        for n in range(0, width, 256):
-            part[s, :, n : n + 256] = dot(hidden[s], down[:, n : n + 256]).astype(jnp.bfloat16)
+    cut = width // CAST
+
+    def part_of(ref, q):
+        return ref.at[:, :, pl.ds(q * cut, cut)]
+
+    def feed_down(q):
+        @pl.loop(0, CAST)
+        def _(s):
+            for n in range(0, cut, 256):
+                part[s, :, q * cut + n : q * cut + n + 256] = dot(
+                    hidden[s], down[q, :, n : n + 256]
+                ).astype(jnp.bfloat16)
+
+    def pair_set(q):
+        return remote(
+            part.at[:, pl.ds(other, half), pl.ds(q * cut, cut)],
+            part_of(pair_two, q),
+            set_send.at[q, 0],
+            set_recv.at[q, 0],
+            partner,
+        )
+
+    def cross_set(q, i):
+        return remote(
+            pair_two.at[peer(i), :, pl.ds(q * cut, cut)],
+            cross_two.at[i - 1, :, pl.ds(q * cut, cut)],
+            set_send.at[q, i],
+            set_recv.at[q, i],
+            at(g, peer(i), t),
+        )
+
+    def sum_set(q):
+        pair_set(q).wait_recv()
+        at_set = pl.ds(q * cut, cut)
+        for i in order:
+            s = peer(i)
+
+            @pl.loop(0, half // STRIP)
+            def _(r):
+                a = part[s, strip(r, mine), at_set].astype(jnp.float32)
+                b = pair_two[s, strip(r), at_set].astype(jnp.float32)
+                pair_two[s, strip(r), at_set] = (a + b).astype(jnp.bfloat16)
+
+            if i:
+                cross_set(q, i).start()
+
+    def finish_set(q):
+        for i in range(1, CAST):
+            cross_set(q, i).wait_recv()
+
+        @pl.loop(0, half // STRIP)
+        def _(r):
+            for plane in range(planes):
+                source = pl.ds(q * cut + plane * depth, depth)
+                target = pl.ds((plane * CAST + q) * depth, depth)
+                value = pair_two[j, strip(r), source].astype(jnp.float32)
+                for i in range(CAST - 1):
+                    value = value + cross_two[i, strip(r), source].astype(jnp.float32)
+                value = value + resid[strip(r), target].astype(jnp.float32)
+                out[strip(r, mine), target] = value.astype(jnp.bfloat16)
 
     def pair(turn, i, buffer):
         s = peer(i)
@@ -479,33 +538,17 @@
     for i in range(1, CAST):
         arrived(i, sec_recv).wait()
         relay(i, secf_send, secf_recv).start()
-    pump(done + 4)
     for i in order:
         relayed(i, secf_recv).wait()
     for i in order:
         feed_up(peer(i))
-    for step in range(done + 5, total):
-        pump(step)
-    for i in order:
-        feed_down(peer(i))
-        pair(1, i, pair_two).start()
-    for i in order:
-        pair_wait(1, i, pair_two)
-        add_pair(i, pair_two)
-        if i:
-            cross(1, i, pair_two, cross_two).start()
-    drain()
-    for i in range(1, CAST):
-        spread(fresh, i, sec_send, sec_recv).wait_send()
-    for i in order:
-        relay(i, secf_send, secf_recv).wait_send()
-    for i in range(1, CAST):
-        cross_wait(1, i, cross_two)
-
-    @pl.loop(0, half // STRIP)
-    def _(r):
-        value = resid[strip(r), :].astype(jnp.float32) + add_cross(r, pair_two, cross_two)
-        out[strip(r, mine), :] = value.astype(jnp.bfloat16)
+    for q in range(CAST):
+        pump(done + 4 + q)
+        feed_down(q)
+        pair_set(q).start()
+        sum_set(q)
+    for q in range(CAST):
+        finish_set(q)
 
     final = remote(
         out.at[pl.ds(mine, half)],
@@ -515,10 +558,15 @@
         partner,
     )
     final.start()
+    drain()
+    for i in range(1, CAST):
+        spread(fresh, i, sec_send, sec_recv).wait_send()
     for i in order:
-        pair(1, i, pair_two).wait_send()
-        if i:
-            cross(1, i, pair_two, cross_two).wait_send()
+        relay(i, secf_send, secf_recv).wait_send()
+    for q in range(CAST):
+        pair_set(q).wait_send()
+        for i in range(1, CAST):
+            cross_set(q, i).wait_send()
     final.wait()
 
 
@@ -551,7 +599,7 @@
             pltpu.VMEM((width, 3 * wide), bf16),
             pltpu.VMEM((wide, width), bf16),
             pltpu.VMEM((width, tall), bf16),
-            pltpu.VMEM((tall, width), bf16),
+            pltpu.VMEM((CAST, tall, width // CAST), bf16),
             pltpu.VMEM((CAST, rows, width), bf16),
             pltpu.VMEM((rows, width), bf16),
             pltpu.VMEM((CAST, rows, tall), bf16),
@@ -573,10 +621,12 @@
             dma((CAST,)),
             dma((CAST,)),
             dma((CAST,)),
-            dma((2, CAST)),
-            dma((2, CAST)),
-            dma((2, CAST)),
-            dma((2, CAST)),
+            dma((1, CAST)),
+            dma((1, CAST)),
+            dma((1, CAST)),
+            dma((1, CAST)),
+            dma((CAST, CAST)),
+            dma((CAST, CAST)),
             dma((1,)),
             dma((1,)),
         ],

time: 274 us -> 267 us (0.974)
  Pallas kernels: 271 us -> 264 us
    pallas_call x1, Pallas kernels: 271 us -> 264 us  [fused(): pl.pallas_call(functools.partial(fused_kernel, planes), out_shape=jax.Sha...]
where the time goes in v2:
time: 267 us
  Pallas kernels  264 us (99%)
  local copies, waits for them, and re-layouts  2.73 us (1%)
    pallas_call x1, Pallas kernels, fused(): pl.pallas_call(functools.partial(fused_kernel, planes), out_shape=jax.Sha...  264 us

profile of v2, /device:TPU:0, one launch (start us, length us, event | category | flops | bytes accessed | tf_op | source)
XLA Modules:
  0.0 267.0 jit_solution(4331571832863504239)
XLA Ops:
  0.0 264.2 %fused_layer.1 = bf16[384,2048]{1,0:T(8,128)(2,1)} custom-call(bf16[384,2048]{1,0:T(8,128)(2,1)} %tokens.1, f32[1,2048]{1,0:T(1,128)} %bitcast.2, bf16[128,1024]{1,0:T(8,128)(2,1)} %w_outer.1, bf16[128,1024]{1,0:T(8,128)(2,1)} %w_inner.1, bf16[128,1024]{1,0:T(8,128)(2,1)} %w_value.1, f32[3,2048]{1,0:T(4,128)} %taps.1, bf16[1024,128]{1,0:T(8,128)(2,1)} %w_mix.1, ...), custom_call_target="tpu_custom_call" | custom-call | tf_op jit(solution)/shard_map/fused_layer/pallas_call | solution.py:593
  264.2 2.7 %copy.12 = bf16[384,2048]{1,0:T(8,128)(2,1)} copy(bf16[384,2048]{1,0:T(8,128)(2,1)} %fused_layer.1) | data formatting | bytes 3145728

commit v3 on v2

--- a/solution.py
+++ b/solution.py
@@ -237,16 +237,17 @@
             place(kind, g, k), place(kind, g, k), swap_recv.at[kind, k]
         ).wait()
 
-    chunks = [(kind, None) for kind in range(4)]
-    chunks += [(4, q) for q in range(CAST)] + [(5, q) for q in range(CAST)]
+    chunks = [((0, 1, 2), None), ((3,), None)]
+    chunks += [((4,), q) for q in range(CAST)] + [((5,), q) for q in range(CAST)]
+    lead = 2
 
     def slab(w, plane):
-        kind, q = chunks[w]
+        kinds, q = chunks[w]
         if q is not None:
-            return place(kind, plane, q)
+            return place(kinds[0], plane, q)
         start = pl.multiple_of(plane * CAST * depth, CAST * depth)
-        if kind < 3:
-            return proj.at[pl.ds(start, CAST * depth), pl.ds(kind * wide, wide)]
+        if len(kinds) > 1:
+            return proj.at[pl.ds(start, CAST * depth), :]
         return mix.at[:, lanes(plane * CAST * depth, CAST * depth)]
 
     def hop(w, plane, up_way):
@@ -264,9 +265,10 @@
             if w < 0 or w >= len(chunks):
                 continue
             if dist == 0:
-                kind, q = chunks[w]
+                kinds, q = chunks[w]
                 for k in range(CAST) if q is None else (q,):
-                    wait_swap(kind, k)
+                    for kind in kinds:
+                        wait_swap(kind, k)
 
                 @pl.when(g < planes - 1)
                 def _():
@@ -359,9 +361,9 @@
         relay(i, fwd_send, fwd_recv).wait_send()
         relayed(i, fwd_recv).wait()
     keep.wait()
-    for step in range(4, 4 + planes - 1):
+    for step in range(4, lead + planes - 1):
         pump(step)
-    done = 4 + planes - 1
+    done = max(lead + planes - 1, 4)
 
     channel = lanes((t * CAST + j) * wide, wide)
     dims = (((1,), (0,)), ((), ()))
@@ -588,7 +590,7 @@
     wide = outer_gate_weight.shape[1] // CAST
     tall = up_projection_weight.shape[1] // CAST
     dma = pltpu.SemaphoreType.DMA
-    chunk_count = 4 + 2 * CAST
+    chunk_count = 2 + 2 * CAST
     bf16 = jnp.bfloat16
     return pl.pallas_call(
         functools.partial(fused_kernel, planes),

time: 267 us -> 269 us (level)
  Pallas kernels: 264 us -> 267 us
where the time goes in v3:
time: 269 us
  Pallas kernels  267 us (99%)
  local copies, waits for them, and re-layouts  2.73 us (1%)
    pallas_call x1, Pallas kernels, fused(): pl.pallas_call(functools.partial(fused_kernel, planes), out_shape=jax.Sha...  267 us

profile of v3, /device:TPU:0, one launch (start us, length us, event | category | flops | bytes accessed | tf_op | source)
XLA Modules:
  0.0 269.2 jit_solution(17236761120637653378)
XLA Ops:
  0.0 266.5 %fused_layer.1 = bf16[384,2048]{1,0:T(8,128)(2,1)} custom-call(bf16[384,2048]{1,0:T(8,128)(2,1)} %tokens.1, f32[1,2048]{1,0:T(1,128)} %bitcast.2, bf16[128,1024]{1,0:T(8,128)(2,1)} %w_outer.1, bf16[128,1024]{1,0:T(8,128)(2,1)} %w_inner.1, bf16[128,1024]{1,0:T(8,128)(2,1)} %w_value.1, f32[3,2048]{1,0:T(4,128)} %taps.1, bf16[1024,128]{1,0:T(8,128)(2,1)} %w_mix.1, ...), custom_call_target="tpu_custom_call" | custom-call | tf_op jit(solution)/shard_map/fused_layer/pallas_call | solution.py:595
  266.5 2.7 %copy.12 = bf16[384,2048]{1,0:T(8,128)(2,1)} copy(bf16[384,2048]{1,0:T(8,128)(2,1)} %fused_layer.1) | data formatting | bytes 3145728
